TPU v7x, 32 devices: a whole 2x2x4 slice. The times are simulated.
32 devices in a mesh: grp: 2 (over y), ep: 8 (over z, core), tp: 2 (over x).
Axes of the slice: x: 2, y: 2, z: 4, core: 2. Of those that a mesh axis runs over, the one named last changes fastest.
Arguments:
- tokens: bfloat16 [2048, 4096], P(('grp', 'ep'), 'tp'), parts along dimension 0, may hold values from -6 to 6
- routes: int32 [2048, 4], P(('grp', 'ep')), parts along dimension 0, may hold values from 0 to 7, all different within a row; in each aligned block of 128 rows (0 to 127, 128 to 255, ...) at most 128 rows name the same one
- route_weights: float32 [2048, 4], P(('grp', 'ep')), parts along dimension 0, may hold values from 0.1 to 1
- norm_gain: float32 [4096], replicated, may hold values from 0.1 to 1.9
- expert_gate: bfloat16 [8, 4096, 1024], P('ep', 'tp'), may hold values from -0.09375 to 0.09375
- expert_up: bfloat16 [8, 4096, 1024], P('ep', 'tp'), may hold values from -0.09375 to 0.09375
- expert_down: bfloat16 [8, 1024, 4096], P('ep', None, 'tp')
- shared_gate: bfloat16 [4096, 1024], P('tp'), may hold values from -0.09375 to 0.09375
- shared_up: bfloat16 [4096, 1024], P('tp'), may hold values from -0.09375 to 0.09375
- shared_down: bfloat16 [1024, 4096], P(None, 'tp')
- out_gain: float32 [4096], P('tp'), may hold values from 0.1 to 1.9
Outputs:
- layer_out: bfloat16 [2048, 4096], P(('grp', 'ep'), 'tp'), parts along dimension 0
There are 2 independent parts, one for each index of `grp`. A program takes and returns all parts, laid end to end along the dimension named above; an argument that names none is the same for every part. Nothing has to cross between parts.
Inputs may be any that keep to these rules, and one draw needn't show every extreme that they name: `routes`: each row names 4 different experts; among the rows of one index of ep no expert is named more than 128 times, and in some such block some expert is named exactly 128 times.
All inputs are finite; a program needn't handle non-finite values.
Results may differ from a plain program's by a relative error of at most 0.023.
Values may be sent and summed in bfloat16 or wider, within the bound.
A program may use at most 64 MiB of HBM per device.

v0:
```python
import jax
import jax.numpy as jnp
from jax import lax
from jax.sharding import PartitionSpec as P

epsilon = 1e-06


def local_product(source, matrix):
    return jnp.dot(source, matrix, preferred_element_type=jnp.float32)


def per_device(
    tokens,
    routes,
    route_weights,
    norm_gain,
    expert_gate,
    expert_up,
    expert_down,
    shared_gate,
    shared_up,
    shared_down,
    out_gain,
):
    block_width = tokens.shape[1]
    full_width = block_width * lax.axis_size("tp")
    width_index = lax.axis_index("tp")
    full_rows = lax.all_gather(tokens, "tp", axis=1, tiled=True)
    full_float = full_rows.astype(jnp.float32)
    normed_full = (
        full_float
        * lax.rsqrt(jnp.mean(full_float * full_float, axis=-1, keepdims=True) + epsilon)
        * norm_gain
    ).astype(jnp.bfloat16)
    normed_block = lax.dynamic_slice_in_dim(normed_full, width_index * block_width, block_width, 1)
    gate_matrix = expert_gate[0]
    up_matrix = expert_up[0]
    down_matrix = expert_down[0]
    experts = lax.axis_size("ep")
    choose = (routes[:, :, None] == jnp.arange(experts, dtype=jnp.int32)[None, None, :]).astype(
        jnp.float32
    )
    weight_table = jnp.sum(route_weights[:, :, None] * choose, axis=1)
    expert_input = lax.all_gather(normed_block, "ep", axis=0, tiled=True)
    table_all = lax.all_gather(weight_table, "ep", axis=0, tiled=True)
    summed = (
        lax.psum(local_product(expert_input, gate_matrix).astype(jnp.bfloat16), "tp").astype(
            jnp.float32
        ),
        lax.psum(local_product(expert_input, up_matrix).astype(jnp.bfloat16), "tp").astype(
            jnp.float32
        ),
        lax.psum(local_product(normed_block, shared_gate).astype(jnp.bfloat16), "tp").astype(
            jnp.float32
        ),
        lax.psum(local_product(normed_block, shared_up).astype(jnp.bfloat16), "tp").astype(
            jnp.float32
        ),
    )
    routed_hidden = (jax.nn.silu(summed[0]) * summed[1]).astype(jnp.bfloat16)
    shared_hidden = (jax.nn.silu(summed[2]) * summed[3]).astype(jnp.bfloat16)
    expert_rows = local_product(routed_hidden, down_matrix).astype(jnp.bfloat16)
    shared_out = local_product(shared_hidden, shared_down)
    own_expert = lax.axis_index("ep")
    column = lax.dynamic_slice_in_dim(table_all, own_expert, 1, 1)
    routed = lax.psum_scatter(
        (column * expert_rows.astype(jnp.float32)).astype(jnp.bfloat16),
        "ep",
        scatter_dimension=0,
        tiled=True,
    ).astype(jnp.float32)
    mixture = routed + shared_out
    square_sum = lax.psum(jnp.sum(mixture * mixture, axis=-1, keepdims=True), "tp")
    scale = lax.rsqrt(square_sum / full_width + epsilon)
    return (mixture * scale * out_gain).astype(jnp.bfloat16)


def solution(mesh):
    return jax.shard_map(
        per_device,
        mesh=mesh,
        in_specs=(
            P(("grp", "ep"), "tp"),
            P(("grp", "ep"), None),
            P(("grp", "ep"), None),
            P(),
            P("ep", "tp", None),
            P("ep", "tp", None),
            P("ep", None, "tp"),
            P("tp", None),
            P("tp", None),
            P(None, "tp"),
            P("tp"),
        ),
        out_specs=P(("grp", "ep"), "tp"),
        check_vma=False,
    )
```

profile of v0, /device:TPU:0, one launch (start us, length us, event | category | flops | bytes accessed | tf_op | source)
XLA Modules:
  0.0 293.4 jit_solution(16838798850096647116)
XLA Ops:
  6.5 0.0 all-gather.3.cloned.1.call-start
  6.5 0.7 all-gather.3.cloned.1.call-update
  7.3 0.0 all-gather.5.cloned.1.call-start
  7.3 0.0 dynamic-slice-start
  7.3 25.6 %all-gather.3.cloned.1.call-done = bf16[128,4096]{1,0:T(8,128)(2,1)} async-done(((bf16[128,2048]{1,0:T(8,128)(2,1)}), bf16[128,4096]{1,0:T(8,128)(2,1)}) %all-gather.3.cloned.1.call-update) | async-done | bytes 1048592 | tf_op jit(solution)/shard_map/all_gather | solution.py:29
  32.9 1.5 multiply_reduce_fusion
  34.4 1.4 convert_element_type.52
  35.9 0.0 dynamic-slice-done
  35.9 1.0 fusion.22
  36.8 0.0 copy-start
  36.8 0.0 all-gather.5.cloned.1.call-update
  36.9 0.0 all-reduce.3.cloned.1.call-start
  36.9 0.0 copy-start.1
  36.9 3.9 %convolution_convert_fusion = bf16[128,1024]{1,0:T(8,128)(2,1)} fusion(bf16[128,2048]{1,0:T(8,128)(2,1)} %fusion.22, bf16[2048,1024]{1,0:T(8,128)(2,1)} %param.19), kind=kOutput, calls=%fused_computation.19 | convolution fusion | flops 537001984 | bytes 4980736 | tf_op jit(solution)/shard_map/dot_general | solution.py:10
  40.8 0.0 copy-done
  40.9 0.0 copy-done.1
  40.9 1.5 convolution_convert_fusion.1
  42.3 41.6 %all-gather.5.cloned.1.call-done = bf16[1024,2048]{1,0:T(8,128)(2,1)} async-done(((bf16[128,2048]{1,0:T(8,128)(2,1)}), bf16[1024,2048]{1,0:T(8,128)(2,1)}) %all-gather.5.cloned.1.call-update) | async-done | bytes 4194320 | tf_op jit(solution)/shard_map/all_gather | solution.py:45
  83.9 0.0 copy-start.5
  83.9 0.0 copy-start.6
  83.9 9.5 %fusion.15 = bf16[1024,1024]{1,0:T(8,128)(2,1)} fusion(bf16[1024,2048]{1,0:T(8,128)(2,1)} %all-gather.5.cloned.1.call-done, bf16[1,2048,1024]{2,1,0:T(8,128)(2,1)} %param.15), kind=kOutput, calls=%fused_computation.17 | convolution fusion | flops 4296015872 | bytes 10485760 | tf_op jit(solution)/shard_map/dot_general | solution.py:10
  93.4 0.0 copy-done.5
  93.4 0.0 copy-done.6
  93.4 5.7 %fusion.18 = bf16[1024,1024]{1,0:T(8,128)(2,1)} fusion(bf16[1024,2048]{1,0:T(8,128)(2,1)S(1)} %copy-done.6, bf16[1,2048,1024]{2,1,0:T(8,128)(2,1)S(1)} %copy-done.5), kind=kOutput, calls=%fused_computation.18 | convolution fusion | flops 4296015872 | bytes 10485760 | tf_op jit(solution)/shard_map/dot_general | solution.py:10
  99.1 0.0 copy-start.3
  99.1 0.0 copy-start.4
  99.1 0.0 all-reduce.3.cloned.1.call-update
  99.1 0.0 reduce-scatter.2.cloned.1.call-start
  99.2 0.6 copy-done.3
  99.8 0.0 copy-done.4
  99.8 14.1 %all_gather.9 = f32[1024,8]{0,1:T(8,128)S(1)} all-gather(f32[128,8]{0,1:T(8,128)S(1)} %select_reduce_fusion), channel_id=1, replica_groups=mesh['grp'=2,'ep'=8,'tp'=2] {'ep'}, dimensions={0}, use_global_device_ids=true | all-gather | bytes 36864 | tf_op jit(solution)/shard_map/all_gather | solution.py:46
  113.9 103.5 %all-reduce.3.cloned.1.call-done = (bf16[1024,1024]{1,0:T(8,128)(2,1)}, bf16[1024,1024]{1,0:T(8,128)(2,1)}, bf16[128,1024]{1,0:T(8,128)(2,1)}, bf16[128,1024]{1,0:T(8,128)(2,1)}) async-done(((bf16[1024,1024]{1,0:T(8,128)(2,1)}, bf16[1024,1024]{1,0:T(8,128)(2,1)}, bf16[128,1024]{1,0:T(8,128)(2,1)}, bf16[128,1024]{1,0:T(8,128)(2,1)}), (bf16[1024,1024]{1,0:T(8,128)(2,1)}, bf16[1024,1024]{1,0:T(8,128)(2,1)}, ...) | async-done | bytes 4718608 | tf_op jit(solution)/shard_map/psum | solution.py:51
  217.4 10.3 %multiply_convert_fusion = bf16[1024,2048]{1,0:T(8,128)(2,1)} fusion(f32[1024]{0:T(1024)S(1)} %bitcast.26, bf16[1,1024,2048]{2,1,0:T(8,128)(2,1)} %param.17, bf16[1024,1024]{1,0:T(8,128)(2,1)} %get-tuple-element.5, bf16[1024,1024]{1,0:T(8,128)(2,1)} %get-tuple-element.6), kind=kOutput, calls=%fused_computation | convolution fusion | flops 4311744512 | bytes 12587008 | tf_op jit(solution)/shard_map/dot_general | solution.py:10
  227.7 0.0 copy-start.7
  227.7 0.0 copy-start.8
  227.7 0.0 reduce-scatter.2.cloned.1.call-update
  227.7 0.0 copy-start.2
  227.7 50.1 %reduce-scatter.2.cloned.1.call-done = bf16[128,2048]{1,0:T(8,128)(2,1)} async-done(((bf16[1024,2048]{1,0:T(8,128)(2,1)}), bf16[128,2048]{1,0:T(8,128)(2,1)}) %reduce-scatter.2.cloned.1.call-update) | async-done | bytes 524304 | tf_op jit(solution)/shard_map/reduce_scatter | solution.py:67
  277.8 0.0 copy-done.7
  277.8 0.0 copy-done.8
  277.8 3.2 %multiply_reduce_fusion.1 = (f32[128]{0:T(128)S(1)}, f32[128,2048]{1,0:T(8,128)S(1)}) fusion(bf16[1024,2048]{1,0:T(8,128)(2,1)} %param.20, bf16[128,1024]{1,0:T(8,128)(2,1)S(1)} %copy-done.7, bf16[128,1024]{1,0:T(8,128)(2,1)S(1)} %copy-done.8, bf16[128,2048]{1,0:T(8,128)(2,1)} %reduce-scatter.2.cloned.1.call-done), kind=kOutput, calls=%fused_computation.25 | convolution fusion | flops 538967936 | bytes 6291968 | tf_op jit(solution)/shard_map/dot_general | solution.py:10
  281.0 4.9 %psum.39 = f32[128,1]{0,1:T(1,128)S(1)} all-reduce(f32[128,1]{0,1:T(1,128)S(1)} %bitcast.27), channel_id=1, replica_groups=mesh['grp'=2,'ep'=8,'tp'=2] {'tp'}, use_global_device_ids=true, to_apply=%region_8.9 | all-reduce | flops 128 | bytes 1024 | tf_op jit(solution)/shard_map/psum | solution.py:74
  285.9 0.0 copy-done.2
  286.0 1.0 multiply_convert_fusion.1
  (4 shorter events, 0.0 us)
Async XLA Ops:
  6.5 26.4 %all-gather.3.cloned.1.call-start = ((), (), s32[]{:S(2)}) async-start(), calls=%async_computation.1 | async-start | bytes 1572864 | tf_op jit(solution)/shard_map/all_gather | solution.py:29
  7.3 76.6 %all-gather.5.cloned.1.call-start = ((), (), s32[]{:S(2)}) async-start(), calls=%async_computation.2 | async-start | bytes 4718592 | tf_op jit(solution)/shard_map/all_gather | solution.py:45
  7.3 28.6 %dynamic-slice-start = ((f32[4096]{0:T(1024)}, s32[]{:T(128)}), f32[2048]{0:T(1024)S(1)}, s32[]{:S(2)}) async-start(f32[4096]{0:T(1024)} %param.14, s32[]{:T(128)} %select_n.7), calls=%async_computation.5 | async-start | bytes 16896 | tf_op jit(solution)/shard_map/dynamic_slice | solution.py:36
  36.8 4.0 %copy-start = (bf16[128,2048]{1,0:T(8,128)(2,1)S(1)}, bf16[128,2048]{1,0:T(8,128)(2,1)}, u32[]{:S(2)}) copy-start(bf16[128,2048]{1,0:T(8,128)(2,1)} %fusion.22) | copy-start | bytes 1572868
  36.9 180.5 %all-reduce.3.cloned.1.call-start = ((), (), s32[]{:S(2)}) async-start(), calls=%async_computation.4 | async-start | bytes 9437184 | tf_op jit(solution)/shard_map/psum | solution.py:51
  36.9 3.9 %copy-start.1 = (bf16[2048,1024]{1,0:T(8,128)(2,1)S(1)}, bf16[2048,1024]{1,0:T(8,128)(2,1)}, u32[]{:S(2)}) copy-start(bf16[2048,1024]{1,0:T(8,128)(2,1)} %param.18) | copy-start | bytes 12582916
  83.9 9.5 %copy-start.5 = (bf16[1,2048,1024]{2,1,0:T(8,128)(2,1)S(1)}, bf16[1,2048,1024]{2,1,0:T(8,128)(2,1)}, u32[]{:S(2)}) copy-start(bf16[1,2048,1024]{2,1,0:T(8,128)(2,1)} %param.16) | copy-start | bytes 12582916
  83.9 9.5 %copy-start.6 = (bf16[1024,2048]{1,0:T(8,128)(2,1)S(1)}, bf16[1024,2048]{1,0:T(8,128)(2,1)}, u32[]{:S(2)}) copy-start(bf16[1024,2048]{1,0:T(8,128)(2,1)} %all-gather.5.cloned.1.call-done) | copy-start | bytes 12582916
  99.1 0.7 copy-start.3
  99.1 0.7 copy-start.4
  99.1 178.7 %reduce-scatter.2.cloned.1.call-start = ((), (), s32[]{:S(2)}) async-start(), calls=%async_computation.3 | async-start | bytes 4718592 | tf_op jit(solution)/shard_map/reduce_scatter | solution.py:67
  227.7 50.1 %copy-start.7 = (bf16[128,1024]{1,0:T(8,128)(2,1)S(1)}, bf16[128,1024]{1,0:T(8,128)(2,1)}, u32[]{:S(2)}) copy-start(bf16[128,1024]{1,0:T(8,128)(2,1)} %get-tuple-element.7) | copy-start | bytes 786436
  227.7 50.1 %copy-start.8 = (bf16[128,1024]{1,0:T(8,128)(2,1)S(1)}, bf16[128,1024]{1,0:T(8,128)(2,1)}, u32[]{:S(2)}) copy-start(bf16[128,1024]{1,0:T(8,128)(2,1)} %get-tuple-element.8) | copy-start | bytes 786436
  227.7 58.2 %copy-start.2 = (f32[2048]{0:T(1024)S(1)}, f32[2048]{0:T(1024)}, u32[]{:S(2)}) copy-start(f32[2048]{0:T(1024)} %param.21) | copy-start | bytes 24580
Sparse Core Ops, SparseCore 0:
  8.9 23.9 all-gather.2
  37.0 46.8 all-gather.4
  99.3 118.0 all-reduce.2
  227.8 49.9 reduce-scatter.1
where the time goes:
time: 294 us; the launch traced here: 293 us
  waiting for transfers between devices  221 us (75%)
  matrix products  34.1 us (12%)
  blocking collectives  19 us (6%)
  between operations  13.2 us (4%)
  other arithmetic  4.88 us (2%)
    psum x1, waiting for transfers between devices, per_device(): lax.psum(local_product(expert_input, up_matrix).astype(jnp.bfloat16), 'tp')  103 us
    reduce_scatter x1, waiting for transfers between devices, per_device(): lax.psum_scatter((column * expert_rows.astype(jnp.float32)).astype(jnp.bf...  50.1 us
    all_gather x1, waiting for transfers between devices, per_device(): expert_input = lax.all_gather(normed_block, 'ep', axis=0, tiled=True)  41.6 us
    dot_general x6, matrix products, local_product(): return jnp.dot(source, matrix, preferred_element_type=jnp.float32)  34.1 us
    all_gather x1, waiting for transfers between devices, per_device(): full_rows = lax.all_gather(tokens, 'tp', axis=1, tiled=True)  25.6 us
    all_gather x1, blocking collectives, per_device(): table_all = lax.all_gather(weight_table, 'ep', axis=0, tiled=True)  14.1 us
  transfers between devices with their start and end apart: 4, of which 4 were waited for; matrix products, arithmetic and copies ran while one was open for 2% of the time, Pallas kernels for 0%

commit v1 on v0

--- a/solution.py
+++ b/solution.py
@@ -26,7 +26,8 @@
     block_width = tokens.shape[1]
     full_width = block_width * lax.axis_size("tp")
     width_index = lax.axis_index("tp")
-    full_rows = lax.all_gather(tokens, "tp", axis=1, tiled=True)
+    parts = lax.all_gather(tokens, "tp")
+    full_rows = jnp.concatenate(parts, axis=1)
     full_float = full_rows.astype(jnp.float32)
     normed_full = (
         full_float

time: 294 us -> 296 us (level)
  no operation moved by 1% of the time
where the time goes in v1:
time: 296 us
  waiting for transfers between devices  222 us (75%)
  matrix products  34.3 us (12%)
  blocking collectives  19.2 us (6%)
  between operations  13.2 us (4%)
  other arithmetic  5.17 us (2%)
    psum x1, waiting for transfers between devices, per_device(): lax.psum(local_product(expert_input, up_matrix).astype(jnp.bfloat16), 'tp')  103 us
    reduce_scatter x1, waiting for transfers between devices, per_device(): lax.psum_scatter((column * expert_rows.astype(jnp.float32)).astype(jnp.bf...  50.1 us
    all_gather x1, waiting for transfers between devices, per_device(): expert_input = lax.all_gather(normed_block, 'ep', axis=0, tiled=True)  42.5 us
    dot_general x6, matrix products, local_product(): return jnp.dot(source, matrix, preferred_element_type=jnp.float32)  34.3 us
    all_gather x1, waiting for transfers between devices, per_device(): parts = lax.all_gather(tokens, 'tp')  25.6 us
    all_gather x1, blocking collectives, per_device(): table_all = lax.all_gather(weight_table, 'ep', axis=0, tiled=True)  14.3 us
  transfers between devices with their start and end apart: 4, of which 4 were waited for; matrix products, arithmetic and copies ran while one was open for 2% of the time, Pallas kernels for 0%

profile of v1, /device:TPU:0, one launch (start us, length us, event | category | flops | bytes accessed | tf_op | source)
XLA Modules:
  0.0 296.1 jit_solution(13095597433880072832)
XLA Ops:
  6.5 0.0 all-gather.6.cloned.1.call-start
  6.5 0.7 all-gather.6.cloned.1.call-update
  7.3 0.0 all-gather.4.cloned.1.call-start
  7.3 0.0 dynamic-slice-start
  7.3 25.6 %all-gather.6.cloned.1.call-done = bf16[256,2048]{1,0:T(8,128)(2,1)} async-done(((bf16[128,2048]{1,0:T(8,128)(2,1)}), bf16[256,2048]{1,0:T(8,128)(2,1)}) %all-gather.6.cloned.1.call-update) | async-done | bytes 1048592 | tf_op jit(solution)/shard_map/all_gather | solution.py:29
  32.9 0.0 copy-start.1
  32.9 1.5 convert_bitcast_fusion
  34.5 1.9 copy.19
  36.3 0.0 copy-done.1
  36.3 0.3 fusion.14
  36.6 0.0 dynamic-slice-done
  36.6 2.4 fusion.23
  39.0 0.0 copy-start
  39.0 0.0 all-gather.4.cloned.1.call-update
  39.0 0.0 all-reduce.3.cloned.1.call-start
  39.1 0.0 copy-start.2
  39.1 3.9 %convolution_convert_fusion = bf16[128,1024]{1,0:T(8,128)(2,1)} fusion(bf16[128,2048]{0,1:T(8,128)(2,1)} %fusion.23, bf16[2048,1024]{1,0:T(8,128)(2,1)} %param.19), kind=kOutput, calls=%fused_computation.21 | convolution fusion | flops 537001984 | bytes 4980736 | tf_op jit(solution)/shard_map/dot_general | solution.py:10
  43.0 0.0 copy-done
  43.0 0.0 copy-done.2
  43.0 1.5 convolution_convert_fusion.1
  44.5 42.5 %all-gather.4.cloned.1.call-done = bf16[1024,2048]{0,1:T(8,128)(2,1)} async-done(((bf16[128,2048]{0,1:T(8,128)(2,1)}), bf16[1024,2048]{0,1:T(8,128)(2,1)}) %all-gather.4.cloned.1.call-update) | async-done | bytes 4194320 | tf_op jit(solution)/shard_map/all_gather | solution.py:46
  87.0 0.0 copy-start.6
  87.0 0.0 copy-start.7
  87.0 9.6 %fusion.16 = bf16[1024,1024]{1,0:T(8,128)(2,1)} fusion(bf16[1024,2048]{0,1:T(8,128)(2,1)} %all-gather.4.cloned.1.call-done, bf16[1,2048,1024]{2,1,0:T(8,128)(2,1)} %param.15), kind=kOutput, calls=%fused_computation.19 | convolution fusion | flops 4296015872 | bytes 10485760 | tf_op jit(solution)/shard_map/dot_general | solution.py:10
  96.6 0.0 copy-done.6
  96.6 0.0 copy-done.7
  96.6 5.8 %fusion.19 = bf16[1024,1024]{1,0:T(8,128)(2,1)} fusion(bf16[1024,2048]{0,1:T(8,128)(2,1)S(1)} %copy-done.7, bf16[1,2048,1024]{2,1,0:T(8,128)(2,1)S(1)} %copy-done.6), kind=kOutput, calls=%fused_computation.20 | convolution fusion | flops 4296015872 | bytes 10485760 | tf_op jit(solution)/shard_map/dot_general | solution.py:10
  102.4 0.0 copy-start.4
  102.4 0.0 copy-start.5
  102.4 0.0 all-reduce.3.cloned.1.call-update
  102.4 0.0 reduce-scatter.2.cloned.1.call-start
  102.5 0.6 copy-done.4
  103.1 0.0 copy-done.5
  103.1 14.3 %all_gather.12 = f32[1024,8]{0,1:T(8,128)S(1)} all-gather(f32[128,8]{0,1:T(8,128)S(1)} %select_reduce_fusion), channel_id=1, replica_groups=mesh['grp'=2,'ep'=8,'tp'=2] {'ep'}, dimensions={0}, use_global_device_ids=true | all-gather | bytes 36864 | tf_op jit(solution)/shard_map/all_gather | solution.py:47
  117.4 102.7 %all-reduce.3.cloned.1.call-done = (bf16[1024,1024]{1,0:T(8,128)(2,1)}, bf16[1024,1024]{1,0:T(8,128)(2,1)}, bf16[128,1024]{1,0:T(8,128)(2,1)}, bf16[128,1024]{1,0:T(8,128)(2,1)}) async-done(((bf16[1024,1024]{1,0:T(8,128)(2,1)}, bf16[1024,1024]{1,0:T(8,128)(2,1)}, bf16[128,1024]{1,0:T(8,128)(2,1)}, bf16[128,1024]{1,0:T(8,128)(2,1)}), (bf16[1024,1024]{1,0:T(8,128)(2,1)}, bf16[1024,1024]{1,0:T(8,128)(2,1)}, ...) | async-done | bytes 4718608 | tf_op jit(solution)/shard_map/psum | solution.py:52
  220.0 10.3 %multiply_convert_fusion = bf16[1024,2048]{1,0:T(8,128)(2,1)} fusion(f32[1024]{0:T(1024)S(1)} %bitcast.34, bf16[1,1024,2048]{2,1,0:T(8,128)(2,1)} %param.17, bf16[1024,1024]{1,0:T(8,128)(2,1)} %get-tuple-element.5, bf16[1024,1024]{1,0:T(8,128)(2,1)} %get-tuple-element.6), kind=kOutput, calls=%fused_computation | convolution fusion | flops 4311744512 | bytes 12587008 | tf_op jit(solution)/shard_map/dot_general | solution.py:10
  230.4 0.0 copy-start.8
  230.4 0.0 copy-start.9
  230.4 0.0 reduce-scatter.2.cloned.1.call-update
  230.4 0.0 copy-start.3
  230.4 50.1 %reduce-scatter.2.cloned.1.call-done = bf16[128,2048]{1,0:T(8,128)(2,1)} async-done(((bf16[1024,2048]{1,0:T(8,128)(2,1)}), bf16[128,2048]{1,0:T(8,128)(2,1)}) %reduce-scatter.2.cloned.1.call-update) | async-done | bytes 524304 | tf_op jit(solution)/shard_map/reduce_scatter | solution.py:68
  280.5 0.0 copy-done.8
  280.5 0.0 copy-done.9
  280.5 3.2 %multiply_reduce_fusion = (f32[128]{0:T(128)S(1)}, f32[128,2048]{1,0:T(8,128)S(1)}) fusion(bf16[1024,2048]{1,0:T(8,128)(2,1)} %param.20, bf16[128,1024]{1,0:T(8,128)(2,1)S(1)} %copy-done.8, bf16[128,1024]{1,0:T(8,128)(2,1)S(1)} %copy-done.9, bf16[128,2048]{1,0:T(8,128)(2,1)} %reduce-scatter.2.cloned.1.call-done), kind=kOutput, calls=%fused_computation.27 | convolution fusion | flops 538967936 | bytes 6291968 | tf_op jit(solution)/shard_map/dot_general | solution.py:10
  283.7 4.9 %psum.39 = f32[128,1]{0,1:T(1,128)S(1)} all-reduce(f32[128,1]{0,1:T(1,128)S(1)} %bitcast.35), channel_id=1, replica_groups=mesh['grp'=2,'ep'=8,'tp'=2] {'tp'}, use_global_device_ids=true, to_apply=%region_8.9 | all-reduce | flops 128 | bytes 1024 | tf_op jit(solution)/shard_map/psum | solution.py:75
  288.6 0.0 copy-done.3
  288.6 1.0 multiply_convert_fusion.1
  (4 shorter events, 0.0 us)
Async XLA Ops:
  6.5 26.4 %all-gather.6.cloned.1.call-start = ((), (), s32[]{:S(2)}) async-start(), calls=%async_computation.3 | async-start | bytes 1572864 | tf_op jit(solution)/shard_map/all_gather | solution.py:29
  7.3 79.7 %all-gather.4.cloned.1.call-start = ((), (), s32[]{:S(2)}) async-start(), calls=%async_computation.1 | async-start | bytes 4718592 | tf_op jit(solution)/shard_map/all_gather | solution.py:46
  7.3 29.3 %dynamic-slice-start = ((f32[4096]{0:T(1024)}, s32[]{:T(128)}), f32[2048]{0:T(1024)S(1)}, s32[]{:S(2)}) async-start(f32[4096]{0:T(1024)} %param.14, s32[]{:T(128)} %select_n.7), calls=%async_computation.5 | async-start | bytes 16896 | tf_op jit(solution)/shard_map/dynamic_slice | solution.py:37
  32.9 3.4 %copy-start.1 = (bf16[256,2048]{1,0:T(8,128)(2,1)S(1)}, bf16[256,2048]{1,0:T(8,128)(2,1)}, u32[]{:S(2)}) copy-start(bf16[256,2048]{1,0:T(8,128)(2,1)} %all-gather.6.cloned.1.call-done) | copy-start | bytes 3145732
  39.0 4.0 %copy-start = (bf16[128,2048]{0,1:T(8,128)(2,1)S(1)}, bf16[128,2048]{0,1:T(8,128)(2,1)}, u32[]{:S(2)}) copy-start(bf16[128,2048]{0,1:T(8,128)(2,1)} %fusion.23) | copy-start | bytes 1572868
  39.0 181.0 %all-reduce.3.cloned.1.call-start = ((), (), s32[]{:S(2)}) async-start(), calls=%async_computation.4 | async-start | bytes 9437184 | tf_op jit(solution)/shard_map/psum | solution.py:52
  39.1 4.0 %copy-start.2 = (bf16[2048,1024]{1,0:T(8,128)(2,1)S(1)}, bf16[2048,1024]{1,0:T(8,128)(2,1)}, u32[]{:S(2)}) copy-start(bf16[2048,1024]{1,0:T(8,128)(2,1)} %param.18) | copy-start | bytes 12582916
  87.0 9.6 %copy-start.6 = (bf16[1,2048,1024]{2,1,0:T(8,128)(2,1)S(1)}, bf16[1,2048,1024]{2,1,0:T(8,128)(2,1)}, u32[]{:S(2)}) copy-start(bf16[1,2048,1024]{2,1,0:T(8,128)(2,1)} %param.16) | copy-start | bytes 12582916
  87.0 9.6 %copy-start.7 = (bf16[1024,2048]{0,1:T(8,128)(2,1)S(1)}, bf16[1024,2048]{0,1:T(8,128)(2,1)}, u32[]{:S(2)}) copy-start(bf16[1024,2048]{0,1:T(8,128)(2,1)} %all-gather.4.cloned.1.call-done) | copy-start | bytes 12582916
  102.4 0.7 copy-start.4
  102.4 0.7 copy-start.5
  102.4 178.1 %reduce-scatter.2.cloned.1.call-start = ((), (), s32[]{:S(2)}) async-start(), calls=%async_computation.2 | async-start | bytes 4718592 | tf_op jit(solution)/shard_map/reduce_scatter | solution.py:68
  230.4 50.1 %copy-start.8 = (bf16[128,1024]{1,0:T(8,128)(2,1)S(1)}, bf16[128,1024]{1,0:T(8,128)(2,1)}, u32[]{:S(2)}) copy-start(bf16[128,1024]{1,0:T(8,128)(2,1)} %get-tuple-element.7) | copy-start | bytes 786436
  230.4 50.1 %copy-start.9 = (bf16[128,1024]{1,0:T(8,128)(2,1)S(1)}, bf16[128,1024]{1,0:T(8,128)(2,1)}, u32[]{:S(2)}) copy-start(bf16[128,1024]{1,0:T(8,128)(2,1)} %get-tuple-element.8) | copy-start | bytes 786436
  230.4 58.2 %copy-start.3 = (f32[2048]{0:T(1024)S(1)}, f32[2048]{0:T(1024)}, u32[]{:S(2)}) copy-start(f32[2048]{0:T(1024)} %param.21) | copy-start | bytes 24580
Sparse Core Ops, SparseCore 0:
  8.9 23.9 all-gather.5
  39.1 47.8 all-gather.3
  102.5 117.4 all-reduce.2
  230.5 49.9 reduce-scatter.1
